TPU v7x, 512 devices: a 4x2x32 block of a 4x8x32 slice. The times are simulated.
512 devices in a mesh: grp: 2 (over y), sp: 32 (over z), dp: 8 (over x, core).
Axes of the slice: x: 4, y: 2, z: 32, core: 2. Of those that a mesh axis runs over, the one named last changes fastest.
The devices are a block of a 4x8x32 slice.
Arguments:
- tokens: bfloat16 [16, 12288, 2048], P(('grp', 'dp'), 'sp'), parts along dimension 0, may hold values from -6 to 6
- w_value: bfloat16 [2048, 1024], P('dp', 'sp'), may hold values from -0.125 to 0.125
- w_gate: bfloat16 [2048, 1024], P('dp', 'sp'), may hold values from -0.125 to 0.125
- conv_weight: bfloat16 [31, 1024], replicated, may hold values from -20 to 20
- norm_gain: float32 [1024], replicated, may hold values from 0.1 to 1.9
- norm_bias: float32 [1024], replicated, may hold values from -3 to 3
- w_out: bfloat16 [1024, 2048], P('sp', 'dp'), may hold values from -0.1875 to 0.1875
Outputs:
- mixed: bfloat16 [16, 12288, 2048], P(('grp', 'dp'), 'sp'), parts along dimension 0
There are 2 independent parts, one for each index of `grp`. A program takes and returns all parts, laid end to end along the dimension named above; an argument that names none is the same for every part. Nothing has to cross between parts.
All inputs are finite; a program needn't handle non-finite values.
Results may differ from a plain program's by a relative error of at most 0.012.
Values may be sent and summed in bfloat16 or wider, within the bound.
No kernel may reach another device: no remote copies, remote signals or barrier semaphores. Data moves between devices by JAX's collectives and lax.ppermute only.
A program may use at most 64 MiB of HBM per device.

v0:
```python
import jax
import jax.numpy as jnp
from jax import lax
from jax.sharding import PartitionSpec as P

EPS = 1e-05


def rows_first(arrays, axis, dims):
    turned = [jnp.moveaxis(a, dim, 0) for a, dim in zip(arrays, dims)]
    both = jnp.concatenate([t.reshape(len(t), -1) for t in turned], axis=1)
    out, at, finished = (lax.all_gather(both, axis, axis=0, tiled=True), 0, [])
    for t, dim in zip(turned, dims):
        share = out[:, at : at + t[0].size].reshape(-1, *t.shape[1:])
        finished.append(jnp.moveaxis(share, 0, dim))
        at += t[0].size
    return tuple(finished)


def passed_along(array, axis, by):
    peers = lax.axis_size(axis)
    pairs = [(i, i + by) for i in range(peers) if 0 <= i + by < peers]
    return lax.ppermute(array, axis, pairs)


def per_device(tokens, w_value, w_gate, conv_weight, norm_gain, norm_bias, w_out):
    pieces = rows_first((w_value, w_gate, w_out), "dp", (0, 0, 1))
    full_value, full_gate, full_out = rows_first((pieces[0], pieces[1], pieces[2]), "sp", (1, 1, 0))
    rows = tokens[0]
    kernel_width = conv_weight.shape[0]
    channels = norm_gain.shape[0]
    value = jnp.dot(rows, full_value, preferred_element_type=jnp.float32)
    gate = jnp.dot(rows, full_gate, preferred_element_type=jnp.float32)
    glu = (value * jax.nn.sigmoid(gate)).astype(jnp.bfloat16)
    earlier = passed_along(glu[rows.shape[0] - (kernel_width - 1) :], "sp", 1)
    extended = jnp.concatenate([earlier, glu], axis=0)
    kernel = conv_weight[::-1][:, None, :]
    conv = lax.conv_general_dilated(
        extended[None],
        kernel,
        (1,),
        [(0, 0)],
        dimension_numbers=("NWC", "WIO", "NWC"),
        feature_group_count=channels,
        preferred_element_type=jnp.float32,
    )[0].astype(jnp.bfloat16)
    conv_f = conv.astype(jnp.float32)
    mean = jnp.mean(conv_f, axis=1, keepdims=True)
    meansq = jnp.mean(conv_f * conv_f, axis=1, keepdims=True)
    scaled = (conv_f - mean) * lax.rsqrt(meansq - mean * mean + EPS) * norm_gain + norm_bias
    normed = jax.nn.silu(scaled).astype(jnp.bfloat16)
    mixed = jnp.dot(normed, full_out, preferred_element_type=jnp.float32)
    return mixed.astype(jnp.bfloat16)[None]


def solution(mesh):
    placed = (
        P(("grp", "dp"), "sp", None),
        P("dp", "sp"),
        P("dp", "sp"),
        P(),
        P(),
        P(),
        P("sp", "dp"),
    )
    return jax.shard_map(
        per_device,
        mesh=mesh,
        in_specs=placed,
        out_specs=P(("grp", "dp"), "sp", None),
        check_vma=False,
    )
```

profile of v0, /device:TPU:34, one launch (start us, length us, event | category | flops | bytes accessed | tf_op | source)
XLA Modules:
  0.0 246.4 jit_solution(5164028319720590578)
XLA Ops:
  6.5 0.0 copy-start
  6.6 0.0 all-gather.2.cloned.1.call-start
  6.6 0.9 pad_maximum_fusion.1
  7.4 50.4 %all_gather.6 = bf16[2048,96]{0,1:T(8,128)(2,1)S(1)} all-gather(bf16[256,96]{0,1:T(8,128)(2,1)S(1)} %pad_maximum_fusion.1), channel_id=1, replica_groups=mesh['grp'=2,'sp'=32,'dp'=8] {'dp'}, dimensions={0}, use_global_device_ids=true | all-gather | bytes 442368 | tf_op jit(solution)/shard_map/all_gather | solution.py:12
  57.9 0.8 pad_maximum_fusion
  58.7 0.1 all-gather.2.cloned.1.call-update
  58.7 153.0 %all-gather.2.cloned.1.call-done = bf16[1024,6144]{1,0:T(8,128)(2,1)} async-done(((bf16[32,6144]{1,0:T(8,128)(2,1)}), bf16[1024,6144]{1,0:T(8,128)(2,1)}) %all-gather.2.cloned.1.call-update) | async-done | bytes 12582928 | tf_op jit(solution)/shard_map/all_gather | solution.py:12
  211.7 0.0 copy-done
  211.7 4.0 %fusion.2 = f32[1024,384]{0,1:T(8,128)S(1)} fusion(bf16[1024,6144]{1,0:T(8,128)(2,1)} %all-gather.2.cloned.1.call-done, bf16[1,384,2048]{2,1,0:T(8,128)(2,1)S(1)} %copy-done), kind=kOutput, calls=%fused_computation.2 | convolution fusion | flops 1610612736 | bytes 7340032 | tf_op jit(solution)/shard_map/dot_general | solution.py:33
  215.7 0.0 copy-start.1
  215.8 4.1 %fusion.30 = bf16[384,1024]{1,0:T(8,128)(2,1)S(1)} fusion(f32[1024,384]{0,1:T(8,128)S(1)} %fusion.2, bf16[1,384,2048]{2,1,0:T(8,128)(2,1)S(1)} %copy-done, bf16[1024,6144]{1,0:T(8,128)(2,1)} %all-gather.2.cloned.1.call-done), kind=kOutput, calls=%fused_computation.28 | convolution fusion | flops 1612578816 | bytes 8126464 | tf_op jit(solution)/shard_map/dot_general | solution.py:32
  219.9 3.0 %collective-permute-start = (bf16[30,1024]{1,0:T(8,128)(2,1)S(1)}, bf16[30,1024]{1,0:T(8,128)(2,1)S(1)}, u32[]{:S(2)}, u32[]{:S(2)}) collective-permute-start(bf16[30,1024]{1,0:T(8,128)(2,1)S(1)} %slice.35), channel_id=1, source_target_pairs={{0,8},{8,16},{16,24},{24,32},{32,40},{40,48},{48,56},{56,64},{64,7... | collective-permute-start | bytes 184328 | tf_op jit(solution)/shard_map/ppermute | solution.py:23
  222.9 0.0 copy-done.1
  222.9 0.3 rev.3
  223.2 1.4 collective-permute-done
  224.6 0.2 maximum_bitcast_fusion
  224.8 0.1 pad
  224.9 0.2 reshape.24
  225.0 0.0 copy-start.4
  225.1 0.5 copy.12
  225.5 0.1 slice.36
  225.7 0.1 copy-done.4
  225.7 3.8 %fusion.37 = f32[8,52,1024]{2,0,1:T(8,128)S(1)} fusion(bf16[1,7,30,1024]{3,1,2,0:T(8,128)(2,1)S(1)} %slice.36, bf16[1,8,52,1024]{3,1,2,0:T(8,128)(2,1)S(1)} %copy.12, pred[8,52]{0,1:T(8,128)(4,1)S(1)} %copy-done.4, bf16[31,1,1024]{2,0,1:T(8,128)(2,1)S(1)} %bitcast.44), kind=kOutput, calls=%fused_computation.29 | convolution fusion | flops 31719424 | bytes 3049888 | tf_op jit(solution)/shard_map/conv_general_dilated | solution.py:38
  229.5 2.3 copy.14
  231.8 1.6 reshape.28
  233.4 0.0 copy-start.2
  233.4 0.0 copy-start.3
  233.4 0.2 fusion.16
  233.6 0.2 slice_reduce_fusion
  233.7 0.3 copy-done.2
  234.0 0.0 copy-done.3
  234.1 5.5 %fusion.10 = bf16[1,384,2048]{2,1,0:T(8,128)(2,1)} fusion(bf16[1024,6144]{1,0:T(8,128)(2,1)} %all-gather.2.cloned.1.call-done, f32[1,416,1024]{2,1,0:T(8,128)S(1)} %reshape.28, f32[1024]{0:T(1024)S(1)} %copy-done.2, f32[1024]{0:T(1024)S(1)} %copy-done.3, f32[384]{0:T(512)S(1)} %get-tuple-element.9, f32[384]{0:T(512)S(1)} %get-tuple-element.8), kind=kOutput, calls=%fused_computation.9 | convolution fusion | flops 1614938112 | bytes 7352320 | tf_op jit(solution)/shard_map/dot_general | solution.py:52
  (3 shorter events, 0.1 us)
Async XLA Ops:
  6.5 205.2 %copy-start = (bf16[1,384,2048]{2,1,0:T(8,128)(2,1)S(1)}, bf16[1,384,2048]{2,1,0:T(8,128)(2,1)}, u32[]{:S(2)}) copy-start(bf16[1,384,2048]{2,1,0:T(8,128)(2,1)} %param.7) | copy-start | bytes 4718596
  6.6 205.2 %all-gather.2.cloned.1.call-start = ((), (), s32[]{:S(2)}) async-start(), calls=%async_computation | async-start | bytes 12976128 | tf_op jit(solution)/shard_map/all_gather | solution.py:12
  215.7 7.2 %copy-start.1 = (bf16[31,1024]{1,0:T(8,128)(2,1)S(1)}, bf16[31,1024]{1,0:T(8,128)(2,1)}, u32[]{:S(2)}) copy-start(bf16[31,1024]{1,0:T(8,128)(2,1)} %param.10) | copy-start | bytes 190468
  219.9 4.7 %collective-permute-start = (bf16[30,1024]{1,0:T(8,128)(2,1)S(1)}, bf16[30,1024]{1,0:T(8,128)(2,1)S(1)}, u32[]{:S(2)}, u32[]{:S(2)}) collective-permute-start(bf16[30,1024]{1,0:T(8,128)(2,1)S(1)} %slice.35), channel_id=1, source_target_pairs={{0,8},{8,16},{16,24},{24,32},{32,40},{40,48},{48,56},{56,64},{64,7... | collective-permute-start | bytes 184328 | tf_op jit(solution)/shard_map/ppermute | solution.py:23
  225.0 0.7 copy-start.4
  233.4 0.7 copy-start.2
  233.4 0.7 copy-start.3
Sparse Core Ops, SparseCore 0:
  58.9 152.8 all-gather.1
where the time goes:
time: 247 us; the launch traced here: 246 us
  waiting for transfers between devices  154 us (62%)
  blocking collectives  50.4 us (20%)
  matrix products  17.4 us (7%)
  between operations  13.6 us (6%)
  local copies, waits for them, and re-layouts  5.38 us (2%)
  starting transfers between devices  2.97 us (1%)
    all_gather x1, waiting for transfers between devices, rows_first(): out, at, finished = (lax.all_gather(both, axis, axis=0, tiled=True), 0, [])  153 us
    all_gather x1, blocking collectives, rows_first(): out, at, finished = (lax.all_gather(both, axis, axis=0, tiled=True), 0, [])  50.4 us
    dot_general x1, matrix products, per_device(): mixed = jnp.dot(normed, full_out, preferred_element_type=jnp.float32)  5.51 us
  transfers between devices with their start and end apart: 2, of which 2 were waited for; matrix products, arithmetic and copies ran while one was open for 0% of the time, Pallas kernels for 0%

commit v1 on v0

--- a/solution.py
+++ b/solution.py
@@ -9,7 +9,13 @@
 def rows_first(arrays, axis, dims):
     turned = [jnp.moveaxis(a, dim, 0) for a, dim in zip(arrays, dims)]
     both = jnp.concatenate([t.reshape(len(t), -1) for t in turned], axis=1)
-    out, at, finished = (lax.all_gather(both, axis, axis=0, tiled=True), 0, [])
+    out, at, finished = (
+        jnp.concatenate(
+            lax.all_to_all(jnp.stack([both] * lax.axis_size(axis)), axis, 0, 0), axis=0
+        ),
+        0,
+        [],
+    )
     for t, dim in zip(turned, dims):
         share = out[:, at : at + t[0].size].reshape(-1, *t.shape[1:])
         finished.append(jnp.moveaxis(share, 0, dim))

time: 247 us -> 1190 us (4.82)
  the two profiles are of different devices: /device:TPU:34 before, /device:TPU:40 now
where the time goes in v1:
time: 1190 us
  blocking collectives  1150 us (97%)
  local copies, waits for them, and re-layouts  14.3 us (1%)
  matrix products  13 us (1%)
    all_to_all x2, blocking collectives, rows_first(): lax.all_to_all(jnp.stack([both] * lax.axis_size(axis)), axis, 0, 0)  1150 us
  transfers between devices with their start and end apart: 1, of which 1 were waited for; matrix products, arithmetic and copies ran while one was open for 0% of the time, Pallas kernels for 0%

profile of v1, /device:TPU:40, one launch (start us, length us, event | category | flops | bytes accessed | tf_op | source)
XLA Modules:
  0.0 1187.2 jit_solution(14321873557777999477)
XLA Ops:
  0.0 0.0 copy-start
  0.0 0.9 pad_maximum_fusion.1
  0.9 13.3 %all_to_all.10 = bf16[8,256,96]{1,2,0:T(8,128)(2,1)S(1)} all-to-all(bf16[8,256,96]{1,2,0:T(8,128)(2,1)S(1)} %stack.4), channel_id=1, replica_groups=mesh['grp'=2,'sp'=32,'dp'=8] {'dp'}, dimensions={0} | all-to-all | bytes 786432 | tf_op jit(solution)/shard_map/all_to_all | solution.py:14
  14.3 6.1 stack.5
  20.4 1138.5 %all_to_all.11 = bf16[32,32,6144]{2,1,0:T(8,128)(2,1)S(1)} all-to-all(bf16[32,32,6144]{2,1,0:T(8,128)(2,1)} %stack.5), channel_id=1, replica_groups=mesh['grp'=2,'sp'=32,'dp'=8] {'sp'}, dimensions={0} | all-to-all | bytes 25165824 | tf_op jit(solution)/shard_map/all_to_all | solution.py:14
  1159.0 0.0 copy-start.1
  1159.0 0.0 copy-done
  1159.0 1.8 fusion.2
  1160.8 2.7 copy-done.1
  1163.5 0.0 copy-start.2
  1163.5 1.9 fusion.30
  1165.5 5.0 collective-permute-start
  1170.5 0.0 copy-done.2
  1170.5 0.3 rev.3
  1170.8 1.4 collective-permute-done
  1172.2 0.2 maximum_bitcast_fusion
  1172.4 0.1 pad
  1172.5 0.2 reshape.36
  1172.6 0.0 copy-start.5
  1172.7 0.5 copy.25
  1173.1 0.1 slice.36
  1173.3 0.1 copy-done.5
  1173.3 3.8 fusion.37
  1177.1 2.3 copy.27
  1179.4 1.6 reshape.40
  1181.0 0.0 copy-start.3
  1181.0 0.0 copy-start.4
  1181.0 0.2 fusion.16
  1181.2 0.2 slice_reduce_fusion
  1181.3 0.3 copy-done.3
  1181.7 0.0 copy-done.4
  1181.7 5.5 fusion.10
  (6 shorter events, 0.1 us)
Async XLA Ops:
  0.0 1159.0 %copy-start = (bf16[1,384,2048]{2,1,0:T(8,128)(2,1)S(1)}, bf16[1,384,2048]{2,1,0:T(8,128)(2,1)}, u32[]{:S(2)}) copy-start(bf16[1,384,2048]{2,1,0:T(8,128)(2,1)} %param.7) | copy-start | bytes 4718596
  1159.0 4.5 copy-start.1
  1163.5 7.0 copy-start.2
  1165.5 6.7 collective-permute-start
  1172.6 0.7 copy-start.5
  1181.0 0.7 copy-start.3
  1181.0 0.7 copy-start.4
